TPU v7x, 512 devices: a whole 4x4x16 slice. The times are simulated.
512 devices in a mesh: ep: 16 (over y, x), tp: 32 (over z, core).
Axes of the slice: x: 4, y: 4, z: 16, core: 2. Of those that a mesh axis runs over, the one named last changes fastest.
Arguments:
- tokens: bfloat16 [3584, 4096], P('ep', 'tp'), may hold values from -6 to 6
- picks: int32 [16, 16, 56], P('ep'), may hold values from 0 to 223, as said below
- pick_weights: float32 [16, 16, 56], P('ep'), may hold values from 0.1 to 1
- gate_weight: bfloat16 [16, 1280, 4096], P('ep', 'tp'), may hold values from -0.09375 to 0.09375
- up_weight: bfloat16 [16, 1280, 4096], P('ep', 'tp'), may hold values from -0.09375 to 0.09375
- down_weight: bfloat16 [16, 1280, 4096], P('ep', None, 'tp'), may hold values from -0.15625 to 0.15625
- dense_gate: bfloat16 [5120, 4096], P('tp'), may hold values from -0.09375 to 0.09375
- dense_up: bfloat16 [5120, 4096], P('tp'), may hold values from -0.09375 to 0.09375
- dense_down: bfloat16 [5120, 4096], P('tp'), may hold values from -0.078125 to 0.078125
- branch_gate: float32 [4096], P('tp'), may hold values from -6 to 6
Outputs:
- mixed: bfloat16 [3584, 4096], P('ep', 'tp')
Inputs may be any that keep to these rules, and one draw needn't show every extreme that they name: For each block s and expert e, the 56 entries picks[s, e, :] are distinct rows of that block.
All inputs are finite; a program needn't handle non-finite values.
Results may differ from a plain program's by a relative error of at most 0.014.
Values may be sent and summed in bfloat16 or wider, within the bound.
No kernel may reach another device: no remote copies, remote signals or barrier semaphores. Data moves between devices by JAX's collectives and lax.ppermute only.
A program may use at most 64 MiB of HBM per device.

v0:
```python
import jax
import jax.numpy as jnp
from jax import lax
from jax.sharding import Mesh
from jax.sharding import PartitionSpec as P

TP = ("tp_0", "tp_1")


def copy_for_each(x, axis):
    copies = jnp.broadcast_to(x, (lax.axis_size(axis), *x.shape))
    return lax.all_to_all(copies, axis, split_axis=0, concat_axis=0, tiled=True)


def laid_out(tiles, dim):
    tiles = jnp.moveaxis(tiles, 0, dim)
    shape = tiles.shape
    return tiles.reshape(*shape[:dim], shape[dim] * shape[dim + 1], *shape[dim + 2 :])


def gather_directly(x, axis, dim):
    tiles = copy_for_each(x, axis)
    return laid_out(tiles, dim)


def stacked_from(x, axes, sequence):
    tiles = x[None]
    for k in sequence:
        tiles = lax.all_gather(tiles, axes[k], axis=0, tiled=True)
    carried = [lax.axis_size(axes[k]) for k in reversed(sequence)]
    tiles = tiles.reshape(*carried, *x.shape)
    turned = sorted(range(len(sequence)), key=lambda place: sequence[len(sequence) - 1 - place])
    return tiles.transpose(*turned, *range(len(sequence), tiles.ndim)).reshape(-1, *x.shape)


def whole_of(x, axes, sequence, dim):
    return laid_out(stacked_from(x, axes, sequence), dim)


def split_up(x, dim, peers):
    shape = x.shape
    tiles = x.reshape(*shape[:dim], peers, shape[dim] // peers, *shape[dim + 1 :])
    return jnp.moveaxis(tiles, dim, 0)


def summed_on_arrival(x, axis, dim):
    peers = lax.axis_size(axis)
    tiles = lax.all_to_all(split_up(x, dim, peers), axis, 0, 0, tiled=True)
    return jnp.sum(tiles.astype(jnp.float32), axis=0)


def per_device(
    tokens,
    picks,
    pick_weights,
    gate_weight,
    up_weight,
    down_weight,
    dense_gate,
    dense_up,
    dense_down,
    branch_gate,
):
    tok_rows = tokens.shape[0]
    experts = picks.shape[1]
    slots = picks.shape[2]
    chosen = picks.reshape(-1)
    full_rows = gather_directly(tokens, TP, 1)
    picked = jnp.take(tokens, chosen, axis=0).reshape(experts, slots, tokens.shape[1])
    landed = lax.all_to_all(picked, "ep", split_axis=0, concat_axis=0, tiled=True)
    arrived = whole_of(landed, TP, (0, 1), 2)
    expert_rows = arrived.reshape(-1, arrived.shape[2])
    contract_last = (((1,), (1,)), ((), ()))
    gate_value = lax.dot_general(
        gate_weight[0], expert_rows, contract_last, preferred_element_type=jnp.float32
    )
    up_value = lax.dot_general(
        up_weight[0], expert_rows, contract_last, preferred_element_type=jnp.float32
    )
    hidden = (jax.nn.silu(gate_value) * up_value).astype(jnp.bfloat16)
    columns = down_weight[0]
    expert_out = lax.dot_general(
        lax.all_gather(hidden, TP, axis=0, tiled=True),
        columns,
        (((0,), (0,)), ((), ())),
        preferred_element_type=jnp.float32,
    ).astype(jnp.bfloat16)
    sent_back = lax.all_to_all(
        expert_out.reshape(-1, slots, columns.shape[1]),
        "ep",
        split_axis=0,
        concat_axis=0,
        tiled=True,
    )
    row_ids = lax.broadcasted_iota(jnp.int32, (experts, tok_rows, slots), 1)
    matches = row_ids == picks[0][:, None, :]
    selector = matches.astype(jnp.bfloat16)
    token_weights = jnp.sum(jnp.where(matches, pick_weights[0][:, None, :], 0.0), axis=2)
    placed = jnp.einsum("ets,esd->etd", selector, sent_back, preferred_element_type=jnp.float32)
    mixture = jnp.sum(token_weights[:, :, None] * placed, axis=0)
    dense_gval = lax.dot_general(
        dense_gate, full_rows, contract_last, preferred_element_type=jnp.float32
    )
    dense_uval = lax.dot_general(
        dense_up, full_rows, contract_last, preferred_element_type=jnp.float32
    )
    dense_hidden = (jax.nn.silu(dense_gval) * dense_uval).astype(jnp.bfloat16)
    dense_part = summed_on_arrival(
        lax.dot_general(
            dense_down, dense_hidden, (((0,), (0,)), ((), ())), preferred_element_type=jnp.float32
        ).astype(jnp.bfloat16),
        TP,
        0,
    )
    mixed = mixture + jax.nn.sigmoid(branch_gate)[None, :] * jnp.transpose(dense_part)
    return mixed.astype(jnp.bfloat16)


def solution(mesh):
    split = Mesh(mesh.devices.reshape(mesh.shape["ep"], 16, 2), ("ep", "tp_0", "tp_1"))
    placed = (
        P("ep", TP),
        P("ep", None, None),
        P("ep", None, None),
        P("ep", TP, None),
        P("ep", TP, None),
        P("ep", None, TP),
        P(TP, None),
        P(TP, None),
        P(TP, None),
        P(TP),
    )
    return jax.shard_map(
        per_device, mesh=split, in_specs=placed, out_specs=P("ep", TP), check_vma=False
    )
```

profile of v0, /device:TPU:1, one launch (start us, length us, event | category | flops | bytes accessed | tf_op | source)
XLA Modules:
  0.0 334.2 jit_solution(6282708274561023143)
XLA Ops:
  6.5 0.0 copy-start
  6.5 0.0 copy-start.1
  6.5 0.0 all-gather.9.cloned.1.call-start
  6.5 0.9 reshape.63
  7.4 0.7 compare_and_fusion
  8.2 2.8 gather_fusion
  11.0 0.2 broadcast_select_fusion
  11.2 15.0 %all_to_all.20 = bf16[16,56,128]{2,1,0:T(8,128)(2,1)} all-to-all(bf16[16,56,128]{2,1,0:T(8,128)(2,1)S(1)} %broadcast_select_fusion), channel_id=1, replica_groups=mesh['ep'=16,'tp_0'=16,'tp_1'=2] {'ep'}, dimensions={0} | all-to-all | bytes 458752 | tf_op jit(solution)/shard_map/all_to_all | solution.py:70
  26.2 0.0 all-gather.9.cloned.1.call-update
  26.2 0.0 copy-done.1
  26.2 1.5 broadcast_in_dim.38
  27.7 17.2 %all-to-all-start.2 = ((bf16[32,224,128]{2,1,0:T(8,128)(2,1)}), bf16[32,224,128]{2,1,0:T(8,128)(2,1)S(1)}, u32[]{:S(2)}, u32[]{:S(2)}) async-start(bf16[32,224,128]{2,1,0:T(8,128)(2,1)} %broadcast_in_dim.38), calls=%async_computation.2 | async-start | bytes 3670016 | tf_op jit(solution)/shard_map/all_to_all | solution.py:12
  44.9 0.0 all-gather.5.cloned.1.call-start
  45.0 124.8 %all-gather.9.cloned.1.call-done = bf16[256,56,128]{2,1,0:T(8,128)(2,1)} async-done(((bf16[16,56,128]{2,1,0:T(8,128)(2,1)}), bf16[256,56,128]{2,1,0:T(8,128)(2,1)}) %all-gather.9.cloned.1.call-update) | async-done | bytes 3670032 | tf_op jit(solution)/shard_map/all_gather | solution.py:29
  169.8 0.0 all-gather.5.cloned.1.call-update
  169.9 0.0 all-to-all-done.2
  169.9 2.1 fusion.8
  172.0 0.0 copy-done
  172.0 4.8 %fusion.12 = bf16[28,32,8,128]{3,2,1,0:T(8,128)(2,1)} fusion(bf16[160,4096]{1,0:T(8,128)(2,1)S(1)} %copy-done, bf16[160,4096]{1,0:T(8,128)(2,1)} %param.17, f32[160,224]{1,0:T(8,128)S(1)} %fusion.8, bf16[32,224,128]{2,1,0:T(8,128)(2,1)S(1)} %all-to-all-done.2), kind=kOutput, calls=%fused_computation.17 | convolution fusion | flops 588335104 | bytes 6434816 | tf_op jit(solution)/shard_map/dot_general | solution.py:109
  176.8 3.1 copy.52
  179.9 13.1 %all-to-all-start.3 = ((bf16[32,128,224]{1,2,0:T(8,128)(2,1)}), bf16[32,128,224]{1,2,0:T(8,128)(2,1)S(1)}, u32[]{:S(2)}, u32[]{:S(2)}) async-start(bf16[32,128,224]{1,2,0:T(8,128)(2,1)} %bitcast.78), calls=%async_computation.3 | async-start | bytes 3670016 | tf_op jit(solution)/shard_map/all_to_all | solution.py:48
  193.0 0.2 all-gather.7.cloned.1.call-start
  193.2 7.0 %all-gather.5.cloned.1.call-done = bf16[32,16,56,128]{3,2,1,0:T(8,128)(2,1)} async-done(((bf16[16,16,56,128]{3,2,1,0:T(8,128)(2,1)}), bf16[32,16,56,128]{3,2,1,0:T(8,128)(2,1)}) %all-gather.5.cloned.1.call-update) | async-done | bytes 7340048 | tf_op jit(solution)/shard_map/all_gather | solution.py:29
  200.2 5.1 %copy.14 = bf16[16,2,16,56,128]{4,3,2,1,0:T(8,128)(2,1)S(1)} copy(bf16[16,2,16,56,128]{4,3,2,0,1:T(8,128)(2,1)} %bitcast.80) | data formatting | bytes 14680064 | tf_op jit(solution)/shard_map/transpose | solution.py:33
  205.3 0.0 copy-start.5
  205.3 7.7 %copy.15 = bf16[16,56,32,128]{3,2,1,0:T(8,128)(2,1)} copy(bf16[16,56,32,128]{3,1,0,2:T(8,128)(2,1)S(1)} %bitcast.79) | data formatting | bytes 14680064 | tf_op jit(solution)/shard_map/transpose | solution.py:16
  213.0 0.0 copy-done.5
  213.0 0.0 copy-start.2
  213.0 0.0 copy-start.6
  213.0 5.5 %fusion.16 = f32[40,896]{1,0:T(8,128)S(1)} fusion(bf16[112,8,32,128]{3,2,1,0:T(8,128)(2,1)} %bitcast.81, bf16[1,40,4096]{2,1,0:T(8,128)(2,1)S(1)} %copy-done.5), kind=kOutput, calls=%fused_computation.20 | convolution fusion | flops 293601280 | bytes 7811072 | tf_op jit(solution)/shard_map/dot_general | solution.py:74
  218.5 0.0 copy-done.2
  218.6 0.0 copy-done.6
  218.6 0.0 copy-start.8
  218.6 0.0 copy-start.7
  218.6 3.0 fusion.28
  221.6 0.0 all-gather.7.cloned.1.call-update
  221.6 0.0 copy-done.8
  221.6 0.0 copy-start.3
  221.6 0.0 copy-start.4
  221.6 88.5 %all-gather.7.cloned.1.call-done = bf16[1280,896]{1,0:T(8,128)(2,1)} async-done(((bf16[40,896]{1,0:T(8,128)(2,1)}), bf16[1280,896]{1,0:T(8,128)(2,1)}) %all-gather.7.cloned.1.call-update) | async-done | bytes 2293776 | tf_op jit(solution)/shard_map/all_gather | solution.py:83
  310.1 0.0 copy-done.7
  310.1 3.2 convolution_convert_fusion.1
  313.3 0.0 all-to-all-done.3
  313.3 4.6 %all-to-all-start.1 = ((bf16[16,56,128]{2,1,0:T(8,128)(2,1)}), bf16[16,56,128]{2,1,0:T(8,128)(2,1)S(1)}, u32[]{:S(2)}, u32[]{:S(2)}) async-start(bf16[16,56,128]{2,1,0:T(8,128)(2,1)} %bitcast.13), calls=%async_computation.1 | async-start | bytes 458752 | tf_op jit(solution)/shard_map/all_to_all | solution.py:88
  317.8 0.0 copy-done.3
  317.8 0.0 copy-done.4
  317.8 0.3 select_reduce_fusion
  318.2 0.3 convert_reduce_fusion
  318.4 7.2 %all-to-all-done.1 = bf16[16,56,128]{2,1,0:T(8,128)(2,1)S(1)} async-done(((bf16[16,56,128]{2,1,0:T(8,128)(2,1)}), bf16[16,56,128]{2,1,0:T(8,128)(2,1)S(1)}, u32[]{:S(2)}, u32[]{:S(2)}) %all-to-all-start.1) | async-done | bytes 229408 | tf_op jit(solution)/shard_map/all_to_all | solution.py:88
  325.7 1.3 multiply_reduce_fusion
  327.0 0.6 fusion.42
  (3 shorter events, 0.0 us)
Async XLA Ops:
  6.5 165.4 %copy-start = (bf16[160,4096]{1,0:T(8,128)(2,1)S(1)}, bf16[160,4096]{1,0:T(8,128)(2,1)}, u32[]{:S(2)}) copy-start(bf16[160,4096]{1,0:T(8,128)(2,1)} %param.18) | copy-start | bytes 3932164
  6.5 19.7 %copy-start.1 = (bf16[224,128]{1,0:T(8,128)(2,1)S(1)}, bf16[224,128]{1,0:T(8,128)(2,1)}, u32[]{:S(2)}) copy-start(bf16[224,128]{1,0:T(8,128)(2,1)} %param.10) | copy-start | bytes 172036
  6.5 163.3 %all-gather.9.cloned.1.call-start = ((), (), s32[]{:S(2)}) async-start(), calls=%async_computation.6 | async-start | bytes 3899392 | tf_op jit(solution)/shard_map/all_gather | solution.py:29
  27.7 142.1 %all-to-all-start.2 = ((bf16[32,224,128]{2,1,0:T(8,128)(2,1)}), bf16[32,224,128]{2,1,0:T(8,128)(2,1)S(1)}, u32[]{:S(2)}, u32[]{:S(2)}) async-start(bf16[32,224,128]{2,1,0:T(8,128)(2,1)} %broadcast_in_dim.38), calls=%async_computation.2 | async-start | bytes 3670016 | tf_op jit(solution)/shard_map/all_to_all | solution.py:12
  44.9 155.3 %all-gather.5.cloned.1.call-start = ((), (), s32[]{:S(2)}) async-start(), calls=%async_computation.4 | async-start | bytes 11010048 | tf_op jit(solution)/shard_map/all_gather | solution.py:29
  179.9 133.4 %all-to-all-start.3 = ((bf16[32,128,224]{1,2,0:T(8,128)(2,1)}), bf16[32,128,224]{1,2,0:T(8,128)(2,1)S(1)}, u32[]{:S(2)}, u32[]{:S(2)}) async-start(bf16[32,128,224]{1,2,0:T(8,128)(2,1)} %bitcast.78), calls=%async_computation.3 | async-start | bytes 3670016 | tf_op jit(solution)/shard_map/all_to_all | solution.py:48
  193.0 117.1 %all-gather.7.cloned.1.call-start = ((), (), s32[]{:S(2)}) async-start(), calls=%async_computation.5 | async-start | bytes 2365440 | tf_op jit(solution)/shard_map/all_gather | solution.py:83
  205.3 7.7 %copy-start.5 = (bf16[1,40,4096]{2,1,0:T(8,128)(2,1)S(1)}, bf16[1,40,4096]{2,1,0:T(8,128)(2,1)}, u32[]{:S(2)}) copy-start(bf16[1,40,4096]{2,1,0:T(8,128)(2,1)} %param.13) | copy-start | bytes 983044
  213.0 5.5 %copy-start.2 = (bf16[16,56,32,128]{3,2,1,0:T(8,128)(2,1)S(1)}, bf16[16,56,32,128]{3,2,1,0:T(8,128)(2,1)}, u32[]{:S(2)}) copy-start(bf16[16,56,32,128]{3,2,1,0:T(8,128)(2,1)} %copy.15) | copy-start | bytes 22020100
  213.0 5.5 %copy-start.6 = (bf16[1,40,4096]{2,1,0:T(8,128)(2,1)S(1)}, bf16[1,40,4096]{2,1,0:T(8,128)(2,1)}, u32[]{:S(2)}) copy-start(bf16[1,40,4096]{2,1,0:T(8,128)(2,1)} %param.14) | copy-start | bytes 983044
  218.6 3.0 copy-start.8
  218.6 91.5 %copy-start.7 = (bf16[1,1280,128]{2,1,0:T(8,128)(2,1)S(1)}, bf16[1,1280,128]{2,1,0:T(8,128)(2,1)}, u32[]{:S(2)}) copy-start(bf16[1,1280,128]{2,1,0:T(8,128)(2,1)} %param.15) | copy-start | bytes 983044
  221.6 96.2 %copy-start.3 = (s32[1,16,56]{2,1,0:T(8,128)S(1)}, s32[1,16,56]{2,1,0:T(8,128)}, u32[]{:S(2)}) copy-start(s32[1,16,56]{2,1,0:T(8,128)} %param.11) | copy-start | bytes 10756
  221.6 96.2 %copy-start.4 = (f32[1,16,56]{2,1,0:T(8,128)S(1)}, f32[1,16,56]{2,1,0:T(8,128)}, u32[]{:S(2)}) copy-start(f32[1,16,56]{2,1,0:T(8,128)} %param.12) | copy-start | bytes 10756
  313.3 12.4 %all-to-all-start.1 = ((bf16[16,56,128]{2,1,0:T(8,128)(2,1)}), bf16[16,56,128]{2,1,0:T(8,128)(2,1)S(1)}, u32[]{:S(2)}, u32[]{:S(2)}) async-start(bf16[16,56,128]{2,1,0:T(8,128)(2,1)} %bitcast.13), calls=%async_computation.1 | async-start | bytes 458752 | tf_op jit(solution)/shard_map/all_to_all | solution.py:88
Sparse Core Ops, SparseCore 0:
  26.3 143.4 all-gather.8
  171.9 28.2 all-gather.4
  221.7 88.3 all-gather.6
where the time goes:
time: 335 us; the launch traced here: 334 us
  waiting for transfers between devices  228 us (68%)
  starting transfers between devices  35.2 us (11%)
  local copies, waits for them, and re-layouts  21.1 us (6%)
  matrix products  19.9 us (6%)
  blocking collectives  15 us (4%)
  between operations  13.3 us (4%)
    all_gather x2, waiting for transfers between devices, stacked_from(): tiles = lax.all_gather(tiles, axes[k], axis=0, tiled=True)  132 us
    all_gather x1, waiting for transfers between devices, per_device(): lax.all_gather(hidden, TP, axis=0, tiled=True)  88.5 us
    all_to_all x1, starting transfers between devices, copy_for_each(): return lax.all_to_all(copies, axis, split_axis=0, concat_axis=0, tiled=True)  17.2 us
    all_to_all x1, blocking collectives, per_device(): lax.all_to_all(picked, 'ep', split_axis=0, concat_axis=0, tiled=True)  15 us
    all_to_all x1, starting transfers between devices, summed_on_arrival(): tiles = lax.all_to_all(split_up(x, dim, peers), axis, 0, 0, tiled=True)  13.1 us
    transpose x1, local copies, waits for them, and re-layouts, laid_out(): tiles = jnp.moveaxis(tiles, 0, dim)  7.66 us
    all_to_all x1, waiting for transfers between devices, per_device(): lax.all_to_all(expert_out.reshape(-1, slots, columns.shape[1]), 'ep', spl...  7.24 us
  transfers between devices with their start and end apart: 6, of which 4 were waited for; matrix products, arithmetic and copies ran while one was open for 11% of the time, Pallas kernels for 0%

commit v1 on v0

--- a/solution.py
+++ b/solution.py
@@ -26,7 +26,9 @@
 def stacked_from(x, axes, sequence):
     tiles = x[None]
     for k in sequence:
-        tiles = lax.all_gather(tiles, axes[k], axis=0, tiled=True)
+        tiles = jnp.concatenate(
+            lax.all_to_all(jnp.stack([tiles] * lax.axis_size(axes[k])), axes[k], 0, 0), axis=0
+        )
     carried = [lax.axis_size(axes[k]) for k in reversed(sequence)]
     tiles = tiles.reshape(*carried, *x.shape)
     turned = sorted(range(len(sequence)), key=lambda place: sequence[len(sequence) - 1 - place])

time: 335 us -> 464 us (1.39)
  blocking collectives: 15 us -> 134 us
  waiting for transfers between devices: 228 us -> 249 us
  starting transfers between devices: 35.2 us -> 19 us
    all_to_all x1, waiting for transfers between devices: 0.01 us -> 149 us  [stacked_from(): lax.all_to_all(jnp.stack([tiles] * lax.axis_size(axes[k])), axes[k], 0, 0)]
    all_gather x2 -> x0, waiting for transfers between devices: 132 us -> none  [stacked_from(): tiles = lax.all_gather(tiles, axes[k], axis=0, tiled=True)]
    all_to_all x0 -> x2, blocking collectives: none -> 119 us  [the longest x1 107 us: copy_for_each(): return lax.all_to_all(copies, axis, split_axis=0, concat_axis=0, tiled=True)]
    all_to_all x1, starting transfers between devices: 17.2 us -> 4.51 us  [stacked_from(): lax.all_to_all(jnp.stack([tiles] * lax.axis_size(axes[k])), axes[k], 0, 0)]
    all_to_all x0 -> x1, local copies, waits for them, and re-layouts: none -> 5.11 us  [stacked_from(): lax.all_to_all(jnp.stack([tiles] * lax.axis_size(axes[k])), axes[k], 0, 0)]
    transpose x1 -> x0, local copies, waits for them, and re-layouts: 5.11 us -> none  [stacked_from(): tiles.transpose(*turned, *range(len(sequence), tiles.ndim))]
  transfers between devices with their start and end apart: 6 -> 4, of which waited for: 4 -> 3; matrix products, arithmetic and copies ran while one was open for 11% -> 8% of each run, Pallas kernels for 0% -> 0%
where the time goes in v1:
time: 464 us; the launch traced here: 463 us
  waiting for transfers between devices  249 us (54%)
  blocking collectives  134 us (29%)
  local copies, waits for them, and re-layouts  22.5 us (5%)
  matrix products  19.9 us (4%)
  starting transfers between devices  19 us (4%)
  between operations  13.6 us (3%)
  other arithmetic  5.98 us (1%)
    all_to_all x1, waiting for transfers between devices, stacked_from(): lax.all_to_all(jnp.stack([tiles] * lax.axis_size(axes[k])), axes[k], 0, 0)  149 us
    all_to_all x1, blocking collectives, copy_for_each(): return lax.all_to_all(copies, axis, split_axis=0, concat_axis=0, tiled=True)  107 us
    all_gather x1, waiting for transfers between devices, per_device(): lax.all_gather(hidden, TP, axis=0, tiled=True)  92.1 us
    all_to_all x1, blocking collectives, per_device(): lax.all_to_all(picked, 'ep', split_axis=0, concat_axis=0, tiled=True)  14.7 us
    all_to_all x1, blocking collectives, stacked_from(): lax.all_to_all(jnp.stack([tiles] * lax.axis_size(axes[k])), axes[k], 0, 0)  12 us
    all_to_all x1, starting transfers between devices, summed_on_arrival(): tiles = lax.all_to_all(split_up(x, dim, peers), axis, 0, 0, tiled=True)  10.7 us
  transfers between devices with their start and end apart: 4, of which 3 were waited for; matrix products, arithmetic and copies ran while one was open for 8% of the time, Pallas kernels for 0%

profile of v1, /device:TPU:1, one launch (start us, length us, event | category | flops | bytes accessed | tf_op | source)
XLA Modules:
  0.0 463.2 jit_solution(11851258625476783091)
XLA Ops:
  6.5 0.0 copy-start
  6.5 0.0 copy-start.1
  6.5 0.9 reshape.62
  7.4 0.7 compare_and_fusion
  8.2 2.8 gather_fusion
  11.0 0.2 broadcast_select_fusion
  11.2 14.7 %all_to_all.30 = bf16[16,56,128]{2,1,0:T(8,128)(2,1)S(1)} all-to-all(bf16[16,56,128]{2,1,0:T(8,128)(2,1)S(1)} %broadcast_select_fusion), channel_id=1, replica_groups=mesh['ep'=16,'tp_0'=16,'tp_1'=2] {'ep'}, dimensions={0} | all-to-all | bytes 458752 | tf_op jit(solution)/shard_map/all_to_all | solution.py:72
  25.9 0.0 copy-done.1
  25.9 0.2 broadcast_in_dim.34
  26.2 106.7 %all_to_all.31 = bf16[32,224,128]{2,1,0:T(8,128)(2,1)S(1)} all-to-all(bf16[32,224,128]{2,1,0:T(8,128)(2,1)S(1)} %broadcast_in_dim.34), channel_id=1, replica_groups=mesh['ep'=16,'tp_0'=16,'tp_1'=2] {'tp_0','tp_1'}, dimensions={0} | all-to-all | bytes 3670016 | tf_op jit(solution)/shard_map/all_to_all | solution.py:12
  132.9 2.6 stack.6
  135.5 4.5 all-to-all-start.1
  140.0 2.1 fusion.8
  142.1 0.0 copy-done
  142.1 4.8 %fusion.12 = bf16[28,32,8,128]{3,2,1,0:T(8,128)(2,1)} fusion(bf16[160,4096]{1,0:T(8,128)(2,1)S(1)} %copy-done, bf16[160,4096]{1,0:T(8,128)(2,1)} %param.17, f32[160,224]{1,0:T(8,128)S(1)} %fusion.8, bf16[32,224,128]{2,1,0:T(8,128)(2,1)S(1)} %all_to_all.31), kind=kOutput, calls=%fused_computation.18 | convolution fusion | flops 588335104 | bytes 6434816 | tf_op jit(solution)/shard_map/dot_general | solution.py:111
  146.9 3.1 copy.50
  150.0 149.3 %all-to-all-done.1 = bf16[16,1,16,56,128]{4,3,2,1,0:T(8,128)(2,1)} async-done(((bf16[16,1,16,56,128]{4,3,2,1,0:T(8,128)(2,1)}), bf16[16,1,16,56,128]{4,3,2,1,0:T(8,128)(2,1)}, u32[]{:S(2)}, u32[]{:S(2)}) %all-to-all-start.1) | async-done | bytes 3670048 | tf_op jit(solution)/shard_map/all_to_all | solution.py:30
  299.3 3.8 pad_maximum_fusion
  303.1 12.0 %all_to_all.32 = bf16[2,16,16,56,128]{4,3,2,1,0:T(8,128)(2,1)} all-to-all(bf16[2,16,16,56,128]{4,3,2,1,0:T(8,128)(2,1)S(1)} %pad_maximum_fusion), channel_id=1, replica_groups=mesh['ep'=16,'tp_0'=16,'tp_1'=2] {'tp_1'}, dimensions={0} | all-to-all | bytes 14680064 | tf_op jit(solution)/shard_map/all_to_all | solution.py:30
  315.2 10.7 %all-to-all-start.5 = ((bf16[32,128,224]{1,2,0:T(8,128)(2,1)}), bf16[32,128,224]{1,2,0:T(8,128)(2,1)S(1)}, u32[]{:S(2)}, u32[]{:S(2)}) async-start(bf16[32,128,224]{1,2,0:T(8,128)(2,1)} %bitcast.77), calls=%async_computation.5 | async-start | bytes 3670016 | tf_op jit(solution)/shard_map/all_to_all | solution.py:50
  325.9 0.2 all-gather.2.cloned.1.call-start
  326.1 5.1 %copy.12 = bf16[2,16,16,56,128]{4,3,2,0,1:T(8,128)(2,1)S(1)} copy(bf16[2,16,16,56,128]{4,3,2,1,0:T(8,128)(2,1)} %all_to_all.32) | data formatting | bytes 14680064 | tf_op jit(solution)/shard_map/all_to_all | solution.py:30
  331.2 0.0 copy-start.5
  331.2 7.7 %copy.13 = bf16[16,56,32,128]{3,2,1,0:T(8,128)(2,1)} copy(bf16[16,56,32,128]{3,1,0,2:T(8,128)(2,1)S(1)} %bitcast.78) | data formatting | bytes 14680064 | tf_op jit(solution)/shard_map/transpose | solution.py:16
  338.9 0.0 copy-done.5
  338.9 0.0 copy-start.2
  338.9 0.0 copy-start.6
  338.9 5.5 %fusion.16 = f32[40,896]{1,0:T(8,128)S(1)} fusion(bf16[112,8,32,128]{3,2,1,0:T(8,128)(2,1)} %bitcast.79, bf16[1,40,4096]{2,1,0:T(8,128)(2,1)S(1)} %copy-done.5), kind=kOutput, calls=%fused_computation.21 | convolution fusion | flops 293601280 | bytes 7811072 | tf_op jit(solution)/shard_map/dot_general | solution.py:76
  344.4 0.0 copy-done.2
  344.4 0.0 copy-done.6
  344.5 0.0 copy-start.8
  344.5 0.0 copy-start.7
  344.5 3.0 fusion.28
  347.4 0.0 all-gather.2.cloned.1.call-update
  347.5 0.0 copy-done.8
  347.5 0.0 copy-start.3
  347.5 0.0 copy-start.4
  347.5 92.1 %all-gather.2.cloned.1.call-done = bf16[1280,896]{1,0:T(8,128)(2,1)} async-done(((bf16[40,896]{1,0:T(8,128)(2,1)}), bf16[1280,896]{1,0:T(8,128)(2,1)}) %all-gather.2.cloned.1.call-update) | async-done | bytes 2293776 | tf_op jit(solution)/shard_map/all_gather | solution.py:85
  439.6 0.0 copy-done.7
  439.6 3.2 convolution_convert_fusion.1
  442.8 0.0 all-to-all-done.5
  442.8 3.5 all-to-all-start.3
  446.3 0.0 copy-done.3
  446.3 0.0 copy-done.4
  446.3 0.3 select_reduce_fusion
  446.7 0.3 convert_reduce_fusion
  446.9 7.5 %all-to-all-done.3 = bf16[16,56,128]{2,1,0:T(8,128)(2,1)S(1)} async-done(((bf16[16,56,128]{2,1,0:T(8,128)(2,1)}), bf16[16,56,128]{2,1,0:T(8,128)(2,1)S(1)}, u32[]{:S(2)}, u32[]{:S(2)}) %all-to-all-start.3) | async-done | bytes 229408 | tf_op jit(solution)/shard_map/all_to_all | solution.py:90
  454.4 1.3 multiply_reduce_fusion
  455.8 0.6 fusion.42
  (3 shorter events, 0.0 us)
Async XLA Ops:
  6.5 135.5 %copy-start = (bf16[160,4096]{1,0:T(8,128)(2,1)S(1)}, bf16[160,4096]{1,0:T(8,128)(2,1)}, u32[]{:S(2)}) copy-start(bf16[160,4096]{1,0:T(8,128)(2,1)} %param.18) | copy-start | bytes 3932164
  6.5 19.4 %copy-start.1 = (bf16[224,128]{1,0:T(8,128)(2,1)S(1)}, bf16[224,128]{1,0:T(8,128)(2,1)}, u32[]{:S(2)}) copy-start(bf16[224,128]{1,0:T(8,128)(2,1)} %param.10) | copy-start | bytes 172036
  135.5 163.8 %all-to-all-start.1 = ((bf16[16,1,16,56,128]{4,3,2,1,0:T(8,128)(2,1)}), bf16[16,1,16,56,128]{4,3,2,1,0:T(8,128)(2,1)}, u32[]{:S(2)}, u32[]{:S(2)}) async-start(bf16[16,1,16,56,128]{4,3,2,1,0:T(8,128)(2,1)} %stack.6), calls=%async_computation.1 | async-start | bytes 7340032 | tf_op jit(solution)/shard_map/all_to_all | solution.py:30
  315.2 127.6 %all-to-all-start.5 = ((bf16[32,128,224]{1,2,0:T(8,128)(2,1)}), bf16[32,128,224]{1,2,0:T(8,128)(2,1)S(1)}, u32[]{:S(2)}, u32[]{:S(2)}) async-start(bf16[32,128,224]{1,2,0:T(8,128)(2,1)} %bitcast.77), calls=%async_computation.5 | async-start | bytes 3670016 | tf_op jit(solution)/shard_map/all_to_all | solution.py:50
  325.9 113.7 %all-gather.2.cloned.1.call-start = ((), (), s32[]{:S(2)}) async-start(), calls=%async_computation.6 | async-start | bytes 2365440 | tf_op jit(solution)/shard_map/all_gather | solution.py:85
  331.2 7.7 %copy-start.5 = (bf16[1,40,4096]{2,1,0:T(8,128)(2,1)S(1)}, bf16[1,40,4096]{2,1,0:T(8,128)(2,1)}, u32[]{:S(2)}) copy-start(bf16[1,40,4096]{2,1,0:T(8,128)(2,1)} %param.13) | copy-start | bytes 983044
  338.9 5.5 %copy-start.2 = (bf16[16,56,32,128]{3,2,1,0:T(8,128)(2,1)S(1)}, bf16[16,56,32,128]{3,2,1,0:T(8,128)(2,1)}, u32[]{:S(2)}) copy-start(bf16[16,56,32,128]{3,2,1,0:T(8,128)(2,1)} %copy.13) | copy-start | bytes 22020100
  338.9 5.5 %copy-start.6 = (bf16[1,40,4096]{2,1,0:T(8,128)(2,1)S(1)}, bf16[1,40,4096]{2,1,0:T(8,128)(2,1)}, u32[]{:S(2)}) copy-start(bf16[1,40,4096]{2,1,0:T(8,128)(2,1)} %param.14) | copy-start | bytes 983044
  344.5 3.0 copy-start.8
  344.5 95.1 %copy-start.7 = (bf16[1,1280,128]{2,1,0:T(8,128)(2,1)S(1)}, bf16[1,1280,128]{2,1,0:T(8,128)(2,1)}, u32[]{:S(2)}) copy-start(bf16[1,1280,128]{2,1,0:T(8,128)(2,1)} %param.15) | copy-start | bytes 983044
  347.5 98.8 %copy-start.3 = (s32[1,16,56]{2,1,0:T(8,128)S(1)}, s32[1,16,56]{2,1,0:T(8,128)}, u32[]{:S(2)}) copy-start(s32[1,16,56]{2,1,0:T(8,128)} %param.11) | copy-start | bytes 10756
  347.5 98.8 %copy-start.4 = (f32[1,16,56]{2,1,0:T(8,128)S(1)}, f32[1,16,56]{2,1,0:T(8,128)}, u32[]{:S(2)}) copy-start(f32[1,16,56]{2,1,0:T(8,128)} %param.12) | copy-start | bytes 10756
  442.8 11.6 %all-to-all-start.3 = ((bf16[16,56,128]{2,1,0:T(8,128)(2,1)}), bf16[16,56,128]{2,1,0:T(8,128)(2,1)S(1)}, u32[]{:S(2)}, u32[]{:S(2)}) async-start(bf16[16,56,128]{2,1,0:T(8,128)(2,1)} %bitcast.12), calls=%async_computation.3 | async-start | bytes 458752 | tf_op jit(solution)/shard_map/all_to_all | solution.py:90
Sparse Core Ops, SparseCore 0:
  347.6 91.9 all-gather.1
